TPU v7x, 32 devices: a whole 2x2x4 slice. The times are simulated.
32 devices in a mesh: ep: 8 (over z, x), tp: 4 (over y, core).
Axes of the slice: x: 2, y: 2, z: 4, core: 2. Of those that a mesh axis runs over, the one named last changes fastest.
Arguments:
- queries: bfloat16 [2048, 8, 128], P('ep', 'tp'), may hold values from -256 to 256
- keys: bfloat16 [2048, 4, 128], P('ep', 'tp'), may hold values from -8 to 8
- values: bfloat16 [2048, 4, 128], P('ep', 'tp'), may hold values from -6 to 6
- attn_lambda: float32 [8], P('tp'), may hold values from 0.3 to 0.8
- head_gain: float32 [128], replicated, may hold values from 0.1 to 1.9
- w_out: bfloat16 [1024, 2048], replicated, may hold values from -0.1875 to 0.1875
- moe_rows: bfloat16 [4096, 2048], P('ep'), may hold values from -6 to 6
- moe_gain: float32 [2048], replicated, may hold values from 0.1 to 1.9
- routes: int32 [4096, 2], P('ep'), may hold values from 0 to 7, all different within a row; in each aligned block of 128 rows (0 to 127, 128 to 255, ...) at most 64 rows name the same one
- route_weights: float32 [4096, 2], P('ep'), may hold values from 0.1 to 1
- w_gate: bfloat16 [8, 2048, 1024], P('ep', None, 'tp'), may hold values from -0.125 to 0.125
- w_up: bfloat16 [8, 2048, 1024], P('ep', None, 'tp'), may hold values from -0.125 to 0.125
- w_down: bfloat16 [8, 1024, 2048], P('ep', 'tp'), may hold values from -0.1875 to 0.1875
Outputs:
- mixer_out: bfloat16 [2048, 2048], P(('ep', 'tp'))
- moe_out: bfloat16 [4096, 2048], P(('ep', 'tp'))
Inputs may be any that keep to these rules, and one draw needn't show every extreme that they name: `routes`: each row names 2 different experts. In each aligned block of 128 rows (the rows of moe_out that one device holds) no expert is named by more than 64 rows, a bound that some block reaches.
All inputs are finite; a program needn't handle non-finite values.
Results may differ from a plain program's by a relative error of at most 0.011.
Values may be sent and summed in bfloat16 or wider, within the bound.
A program may use at most 128 MiB of HBM per device.

v0:
```python
import jax
import jax.numpy as jnp
from jax import lax
from jax.sharding import PartitionSpec as P

EPSILON = 1e-06
MASKED = -1e30


def rms_scaled(values_f, gain):
    mean_sq = jnp.mean(values_f * values_f, axis=-1, keepdims=True)
    return values_f * lax.rsqrt(mean_sq + EPSILON) * gain


def slot_numbers(block_routes, experts):
    flat_ids = block_routes.reshape(-1)
    matches = (flat_ids[:, None] == lax.iota(jnp.int32, experts)[None, :]).astype(jnp.int32)
    earlier = jnp.cumsum(matches, axis=0) - matches
    return jnp.sum(earlier * matches, axis=1).reshape(block_routes.shape)


def fill_slots(block_rows, block_routes, experts, capacity):
    slot_ids = slot_numbers(block_routes, experts)
    model_width = block_rows.shape[1]
    copies = jnp.broadcast_to(block_rows[:, None, :], block_routes.shape + (model_width,))
    blank_slots = jnp.zeros((experts, capacity, model_width), block_rows.dtype)
    return (blank_slots.at[block_routes, slot_ids].set(copies), slot_ids)


def local(
    queries,
    keys,
    values,
    attn_lambda,
    head_gain,
    w_out,
    moe_rows,
    moe_gain,
    routes,
    route_weights,
    w_gate,
    w_up,
    w_down,
):
    positions = queries.shape[0]
    q_heads = queries.shape[1]
    kv_heads = keys.shape[1]
    head_dim = queries.shape[2] // 2
    value_dim = values.shape[2]
    per_key = q_heads // kv_heads
    first_pos = lax.axis_index("ep") * positions
    query_pos = first_pos + lax.iota(jnp.int32, positions)
    last_pos = first_pos + positions - 1
    query_view = queries.reshape(positions, kv_heads, per_key, 2, head_dim)
    inv_scale = head_dim ** (-0.5)
    start_max = jnp.full((positions, kv_heads, per_key, 2), MASKED, jnp.float32)
    start_total = jnp.zeros((positions, kv_heads, per_key, 2), jnp.float32)
    start_acc = jnp.zeros((positions, kv_heads, per_key, 2, value_dim), jnp.float32)
    carry = (start_max, start_total, start_acc)
    key_piece = lax.all_gather(keys, "ep", axis=0, tiled=True)
    value_piece = lax.all_gather(values, "ep", axis=0, tiled=True)
    shard_count = key_piece.shape[0] // positions
    together = 1
    for candidate in (2, 3, 4):
        if shard_count % candidate == 0:
            together = candidate
    block_len = together * positions
    blocks = shard_count // together
    key_blocks = key_piece.reshape(blocks, block_len, kv_heads, 2, head_dim)
    value_blocks = value_piece.reshape(blocks, block_len, kv_heads, value_dim)
    block_starts = block_len * lax.iota(jnp.int32, blocks)

    def visit(running, inputs):
        key_blk, value_blk, block_start = inputs

        def update(current):
            run_max, run_total, run_acc = current
            key_pos = block_start + lax.iota(jnp.int32, block_len)
            scores = (
                jnp.einsum(
                    "qkgmd,pkmd->qkgmp", query_view, key_blk, preferred_element_type=jnp.float32
                )
                * inv_scale
            )
            allowed = key_pos[None, :] <= query_pos[:, None]
            scores = jnp.where(allowed[:, None, None, None, :], scores, MASKED)
            new_max = jnp.maximum(run_max, jnp.max(scores, axis=-1))
            shrink = jnp.exp(run_max - new_max)
            weights = jnp.exp(scores - new_max[..., None])
            run_total = run_total * shrink + jnp.sum(weights, axis=-1)
            run_acc = run_acc * shrink[..., None] + jnp.einsum(
                "qkgmp,pkv->qkgmv",
                weights.astype(jnp.bfloat16),
                value_blk,
                preferred_element_type=jnp.float32,
            )
            return (new_max, run_total, run_acc)

        def keep(current):
            return current

        return (lax.cond(block_start <= last_pos, update, keep, running), None)

    carry, unused = lax.scan(visit, carry, (key_blocks, value_blocks, block_starts))
    run_max, run_total, run_acc = carry
    ratios = run_acc / run_total[..., None]
    lambda_view = attn_lambda.reshape(1, kv_heads, per_key, 1)
    head_out = ratios[:, :, :, 0] - lambda_view * ratios[:, :, :, 1]
    attn_rows = (
        rms_scaled(head_out, head_gain).astype(jnp.bfloat16).reshape(positions, q_heads * value_dim)
    )
    tp_count = lax.axis_size("tp")
    tp_id = lax.axis_index("tp")
    exchanged = lax.all_to_all(
        attn_rows.reshape(positions, q_heads, value_dim),
        "tp",
        split_axis=0,
        concat_axis=1,
        tiled=True,
    )
    mixer_out = jnp.dot(
        exchanged.reshape(positions // tp_count, tp_count * q_heads * value_dim),
        w_out,
        preferred_element_type=jnp.float32,
    ).astype(jnp.bfloat16)
    experts = lax.axis_size("ep")
    dev_rows = moe_rows.shape[0] // tp_count
    top_count = routes.shape[1]
    capacity = max(2, 2 * dev_rows * top_count // experts)
    model_width = moe_rows.shape[1]
    hidden_units = w_gate.shape[2]
    own_routes = lax.dynamic_slice_in_dim(routes, tp_id * dev_rows, dev_rows, 0)
    own_weights = lax.dynamic_slice_in_dim(route_weights, tp_id * dev_rows, dev_rows, 0)
    own_rows = rms_scaled(
        lax.dynamic_slice_in_dim(moe_rows, tp_id * dev_rows, dev_rows, 0).astype(jnp.float32),
        moe_gain,
    ).astype(jnp.bfloat16)
    outgoing, own_slots = fill_slots(own_rows, own_routes, experts, capacity)
    arrived = lax.all_to_all(outgoing, "ep", split_axis=0, concat_axis=0, tiled=True)
    slot_rows = lax.all_gather(arrived[None], "tp", axis=0, tiled=True)
    flat_rows = slot_rows.reshape(-1, model_width)
    gate_out = jnp.dot(flat_rows, w_gate[0], preferred_element_type=jnp.float32)
    up_out = jnp.dot(flat_rows, w_up[0], preferred_element_type=jnp.float32)
    hidden = (
        (jax.nn.silu(gate_out) * up_out)
        .astype(jnp.bfloat16)
        .reshape(slot_rows.shape[:-1] + (hidden_units,))
    )
    flat_terms = hidden.reshape(-1, hidden_units)
    summed = lax.psum_scatter(
        jnp.dot(flat_terms, w_down[0], preferred_element_type=jnp.float32)
        .reshape(hidden.shape[:-1] + (model_width,))
        .astype(jnp.bfloat16),
        "tp",
        scatter_dimension=0,
        tiled=True,
    )
    returned = lax.all_to_all(summed, "ep", split_axis=1, concat_axis=1, tiled=True)[0]
    picked = returned[own_routes, own_slots]
    moe_out = jnp.sum(own_weights[..., None] * picked.astype(jnp.float32), axis=1).astype(
        jnp.bfloat16
    )
    return (mixer_out, moe_out)


def solution(mesh):
    return jax.shard_map(
        local,
        mesh=mesh,
        in_specs=(
            P("ep", "tp", None),
            P("ep", "tp", None),
            P("ep", "tp", None),
            P("tp"),
            P(),
            P(),
            P("ep", None),
            P(),
            P("ep", None),
            P("ep", None),
            P("ep", None, "tp"),
            P("ep", None, "tp"),
            P("ep", "tp", None),
        ),
        out_specs=(P(("ep", "tp"), None), P(("ep", "tp"), None)),
        check_vma=False,
    )
```

profile of v0, /device:TPU:0, one launch (start us, length us, event | category | flops | bytes accessed | tf_op | source)
XLA Modules:
  0.0 330.0 jit_solution(4695768976303798606)
XLA Ops:
  7.2 0.8 constant_dynamic-slice_fusion
  8.1 0.1 eq.29
  8.2 0.1 eq.25
  8.4 0.6 reduce-window.6
  9.0 0.2 slice_reduce_fusion
  9.3 0.1 reshape.223
  9.5 0.1 reshape.231
  9.7 1.2 fusion.24
  10.9 1.3 fusion.26
  12.2 0.6 broadcast_in_dim.60
  12.8 1.2 reshape.233
  14.1 0.2 broadcast_in_dim.58
  14.3 33.4 %scatter_fusion = bf16[8,64,2048]{2,1,0:T(8,128)(2,1)S(1)} fusion(bf16[8,64,2048]{2,1,0:T(8,128)(2,1)S(1)} %broadcast_in_dim.58, s32[256]{0:T(256)S(1)} %reshape.231, bf16[256,2048]{1,0:T(8,128)(2,1)} %reshape.233), kind=kCustom, calls=%fused_computation.1 | custom fusion | bytes 3147776 | tf_op jit(solution)/shard_map/scatter | solution.py:27
  47.7 55.4 %all_to_all.25 = bf16[8,64,2048]{2,1,0:T(8,128)(2,1)} all-to-all(bf16[8,64,2048]{2,1,0:T(8,128)(2,1)S(1)} %scatter_fusion), channel_id=1, replica_groups=mesh['ep'=8,'tp'=4] {'ep'}, dimensions={0} | all-to-all | bytes 4194304 | tf_op jit(solution)/shard_map/all_to_all | solution.py:139
  103.2 57.4 %all-gather.3.cloned.1.call-done = bf16[32,64,2048]{2,1,0:T(8,128)(2,1)} async-done(((bf16[8,64,2048]{2,1,0:T(8,128)(2,1)}), bf16[32,64,2048]{2,1,0:T(8,128)(2,1)}) %all-gather.3.cloned.1.call-update) | async-done | bytes 8388624 | tf_op jit(solution)/shard_map/all_gather | solution.py:140
  160.6 5.9 %fusion.29 = f32[2048,256]{1,0:T(8,128)S(1)} fusion(bf16[2048,2048]{1,0:T(8,128)(2,1)} %bitcast.134, bf16[1,2048,256]{2,1,0:T(8,128)(2,1)S(1)} %copy-done.7), kind=kOutput, calls=%fused_computation.40 | convolution fusion | flops 2147483648 | bytes 11534336 | tf_op jit(solution)/shard_map/dot_general | solution.py:142
  166.6 2.6 fusion.23
  169.2 5.6 %convolution_convert_fusion = bf16[4,8,64,2048]{3,2,1,0:T(8,128)(2,1)} fusion(bf16[4,8,64,256]{3,2,1,0:T(8,128)(2,1)S(1)} %bitcast.130, bf16[1,256,2048]{2,1,0:T(8,128)(2,1)S(1)} %copy-done), kind=kOutput, calls=%fused_computation.28 | convolution fusion | flops 2151677952 | bytes 10485760 | tf_op jit(solution)/shard_map/dot_general | solution.py:151
  174.8 0.8 copy-done.2
  175.6 31.4 %all_gather.9 = bf16[2048,1,128]{2,0,1:T(8,128)(2,1)S(1)} all-gather(bf16[256,1,128]{2,0,1:T(8,128)(2,1)S(1)} %copy-done.2), channel_id=1, replica_groups=mesh['ep'=8,'tp'=4] {'ep'}, dimensions={0}, use_global_device_ids=true | all-gather | bytes 589824 | tf_op jit(solution)/shard_map/all_gather | solution.py:60
  207.1 0.4 reshape.243
  207.5 0.7 copy.64
  208.3 31.4 %all_gather.10 = bf16[2048,1,128]{2,0,1:T(8,128)(2,1)S(1)} all-gather(bf16[256,1,128]{2,0,1:T(8,128)(2,1)S(1)} %copy-done.3), channel_id=1, replica_groups=mesh['ep'=8,'tp'=4] {'ep'}, dimensions={0}, use_global_device_ids=true | all-gather | bytes 589824 | tf_op jit(solution)/shard_map/all_gather | solution.py:61
  239.7 0.2 copy.66
  240.1 5.6 %while.15 = (s32[]{:T(128)}, f32[256,1,2,2]{0,2,3,1:T(2,128)S(1)}, f32[256,1,2,2]{0,2,3,1:T(2,128)S(1)}, f32[256,1,2,2,128]{0,4,3,2,1:T(8,128)S(1)}, s32[2]{0:T(...) while((s32[]{:T(128)}, f32[256,1,2,2]{0,2,3,1:T(2,128)S(1)}, ...), condition=%wide.region_5.6_spmd.clone, body=%wide.region_0.5_spmd.clone.sunk | while | flops 411570432 | bytes 15155487 | solution.py:104
  240.2 0.6 dynamic_slice.50
  241.3 3.3 conditional.3
  241.3 0.6 iota_add_fusion
  241.9 0.2 broadcast_compare_fusion
  242.1 0.9 fusion.4
  243.0 1.0 fusion.5
  244.0 0.5 fusion.11
  244.6 0.6 dynamic_slice.50
  245.8 0.2 copy.68
  246.0 0.1 copy.67
  246.1 0.7 broadcast_divide_fusion
  246.9 0.4 fusion.33
  247.4 0.4 fusion.37
  247.8 7.0 %all_to_all.26 = bf16[256,2,128]{2,1,0:T(2,128)(2,1)S(1)} all-to-all(bf16[256,2,128]{2,1,0:T(2,128)(2,1)S(1)} %fusion.37), channel_id=1, replica_groups=mesh['ep'=8,'tp'=4] {'tp'}, dimensions={0} | all-to-all | bytes 262144 | tf_op jit(solution)/shard_map/all_to_all | solution.py:114
  254.8 8.9 %all-to-all-start.2 = ((bf16[1,8,64,2048]{3,2,0,1:T(8,128)(2,1)}), bf16[1,8,64,2048]{3,2,0,1:T(8,128)(2,1)S(1)}, u32[]{:S(2)}, u32[]{:S(2)}) async-start(bf16[1,8,64,2048]{3,2,0,1:T(8,128)(2,1)} %bitcast.127), calls=%async_computation.3 | async-start | bytes 4194304 | tf_op jit(solution)/shard_map/all_to_all | solution.py:158
  263.7 0.1 reshape.225
  263.9 0.7 constant_dynamic-slice_fusion.1
  264.7 0.1 copy.72
  264.9 3.7 %convolution_convert_fusion.1 = bf16[64,2048]{1,0:T(8,128)(2,1)} fusion(bf16[64,1024]{1,0:T(8,128)(2,1)S(1)} %reshape.221, bf16[1024,2048]{1,0:T(8,128)(2,1)} %param.22), kind=kOutput, calls=%fused_computation.31 | convolution fusion | flops 268566528 | bytes 4587520 | tf_op jit(solution)/shard_map/dot_general | solution.py:121
  268.6 42.9 %all-to-all-done.2 = bf16[1,8,64,2048]{3,2,0,1:T(8,128)(2,1)S(1)} async-done(((bf16[1,8,64,2048]{3,2,0,1:T(8,128)(2,1)}), bf16[1,8,64,2048]{3,2,0,1:T(8,128)(2,1)S(1)}, u32[]{:S(2)}, u32[]{:S(2)}) %all-to-all-start.2) | async-done | bytes 2097184 | tf_op jit(solution)/shard_map/all_to_all | solution.py:158
  311.6 5.3 %gather_fusion = bf16[256,2048]{1,0:T(8,128)(2,1)} fusion(bf16[8,64,2048]{2,1,0:T(8,128)(2,1)S(1)} %bitcast.126, s32[256]{0:T(256)S(1)} %reshape.225), kind=kCustom, calls=%fused_computation | custom fusion | bytes 2099200 | tf_op jit(solution)/shard_map/gather | solution.py:159
  316.9 2.4 reshape.239
  319.3 3.9 %multiply_reduce_fusion = bf16[128,2048]{1,0:T(8,128)(2,1)} fusion(f32[128,2,2048]{2,1,0:T(2,128)S(1)} %reshape.239, f32[128,2]{1,0:T(8,128)S(1)} %copy.73), kind=kLoop, calls=%fused_computation.32 | loop fusion | flops 786432 | bytes 2622464 | tf_op jit(solution)/shard_map/reduce_sum | solution.py:160
  (47 shorter events, 1.0 us)
Async XLA Ops:
  7.2 162.1 %copy-start = (bf16[1,256,2048]{2,1,0:T(8,128)(2,1)S(1)}, bf16[1,256,2048]{2,1,0:T(8,128)(2,1)}, u32[]{:S(2)}) copy-start(bf16[1,256,2048]{2,1,0:T(8,128)(2,1)} %param.29) | copy-start | bytes 3145732
  7.2 153.4 %all-gather.3.cloned.1.call-start = ((), (), s32[]{:S(2)}) async-start(), calls=%async_computation.5 | async-start | bytes 10485760 | tf_op jit(solution)/shard_map/all_gather | solution.py:140
  103.1 57.5 %copy-start.7 = (bf16[1,2048,256]{2,1,0:T(8,128)(2,1)S(1)}, bf16[1,2048,256]{2,1,0:T(8,128)(2,1)}, u32[]{:S(2)}) copy-start(bf16[1,2048,256]{2,1,0:T(8,128)(2,1)} %param.27) | copy-start | bytes 3145732
  103.1 151.7 %reduce-scatter.2.cloned.1.call-start = ((), (), s32[]{:S(2)}) async-start(), calls=%async_computation.4 | async-start | bytes 10485760 | tf_op jit(solution)/shard_map/reduce_scatter | solution.py:150
  160.6 5.9 %copy-start.6 = (bf16[32,64,2048]{2,1,0:T(8,128)(2,1)S(1)}, bf16[32,64,2048]{2,1,0:T(8,128)(2,1)}, u32[]{:S(2)}) copy-start(bf16[32,64,2048]{2,1,0:T(8,128)(2,1)} %all-gather.3.cloned.1.call-done) | copy-start | bytes 25165828
  160.6 6.0 %copy-start.8 = (bf16[1,2048,256]{2,1,0:T(8,128)(2,1)S(1)}, bf16[1,2048,256]{2,1,0:T(8,128)(2,1)}, u32[]{:S(2)}) copy-start(bf16[1,2048,256]{2,1,0:T(8,128)(2,1)} %param.28) | copy-start | bytes 3145732
  174.8 0.8 copy-start.2
  174.8 33.4 %copy-start.3 = (bf16[256,1,128]{2,0,1:T(8,128)(2,1)S(1)}, bf16[256,1,128]{2,0,1:T(8,128)(2,1)}, u32[]{:S(2)}) copy-start(bf16[256,1,128]{2,0,1:T(8,128)(2,1)} %param.19) | copy-start | bytes 196612
  207.1 32.8 %copy-start.1 = (bf16[256,2,128]{2,1,0:T(2,128)(2,1)S(1)}, bf16[256,2,128]{2,1,0:T(2,128)(2,1)}, u32[]{:S(2)}) copy-start(bf16[256,2,128]{2,1,0:T(2,128)(2,1)} %param.17) | copy-start | bytes 393220
  245.7 1.1 copy-start.4
  245.7 1.6 copy-start.5
  254.8 56.8 %all-to-all-start.2 = ((bf16[1,8,64,2048]{3,2,0,1:T(8,128)(2,1)}), bf16[1,8,64,2048]{3,2,0,1:T(8,128)(2,1)S(1)}, u32[]{:S(2)}, u32[]{:S(2)}) async-start(bf16[1,8,64,2048]{3,2,0,1:T(8,128)(2,1)} %bitcast.127), calls=%async_computation.3 | async-start | bytes 4194304 | tf_op jit(solution)/shard_map/all_to_all | solution.py:158
Sparse Core Ops, SparseCore 0:
  103.2 57.2 all-gather.2
  174.9 71.3 reduce-scatter.1
where the time goes:
time: 331 us; the launch traced here: 330 us
  blocking collectives  125 us (38%)
  waiting for transfers between devices  100 us (30%)
  local copies, waits for them, and re-layouts  49.9 us (15%)
  matrix products  19.2 us (6%)
  between operations  14.4 us (4%)
  other arithmetic  10.6 us (3%)
  starting transfers between devices  9.02 us (3%)
    all_gather x1, waiting for transfers between devices, local(): slot_rows = lax.all_gather(arrived[None], 'tp', axis=0, tiled=True)  57.4 us
    all_to_all x1, blocking collectives, local(): lax.all_to_all(outgoing, 'ep', split_axis=0, concat_axis=0, tiled=True)  55.4 us
    all_to_all x1, waiting for transfers between devices, local(): lax.all_to_all(summed, 'ep', split_axis=1, concat_axis=1, tiled=True)[0]  42.9 us
    scatter x1, local copies, waits for them, and re-layouts, fill_slots(): return (blank_slots.at[block_routes, slot_ids].set(copies), slot_ids)  33.4 us
    all_gather x1, blocking collectives, local(): key_piece = lax.all_gather(keys, 'ep', axis=0, tiled=True)  31.4 us
    all_gather x1, blocking collectives, local(): value_piece = lax.all_gather(values, 'ep', axis=0, tiled=True)  31.4 us
    all_to_all x1, starting transfers between devices, local(): lax.all_to_all(summed, 'ep', split_axis=1, concat_axis=1, tiled=True)[0]  8.94 us
    all_to_all x1, blocking collectives, local(): lax.all_to_all(attn_rows.reshape(positions, q_heads, value_dim), 'tp', sp...  6.99 us
  transfers between devices with their start and end apart: 3, of which 2 were waited for; matrix products, arithmetic and copies ran while one was open for 4% of the time, Pallas kernels for 0%

commit v1 on v0

--- a/solution.py
+++ b/solution.py
@@ -137,7 +137,12 @@
     ).astype(jnp.bfloat16)
     outgoing, own_slots = fill_slots(own_rows, own_routes, experts, capacity)
     arrived = lax.all_to_all(outgoing, "ep", split_axis=0, concat_axis=0, tiled=True)
-    slot_rows = lax.all_gather(arrived[None], "tp", axis=0, tiled=True)
+    ring = [arrived[None]]
+    for hop in range(3):
+        ring.append(lax.ppermute(ring[-1], "tp", [(dev, (dev + 1) % 4) for dev in range(4)]))
+    slot_rows = jnp.roll(
+        jnp.concatenate(ring[::-1], axis=0), (lax.axis_index("tp") + 1) * ring[0].shape[0], axis=0
+    )
     flat_rows = slot_rows.reshape(-1, model_width)
     gate_out = jnp.dot(flat_rows, w_gate[0], preferred_element_type=jnp.float32)
     up_out = jnp.dot(flat_rows, w_up[0], preferred_element_type=jnp.float32)

time: 331 us -> 378 us (1.14)
  local copies, waits for them, and re-layouts: 49.9 us -> 78.3 us
  waiting for transfers between devices: 100 us -> 120 us
    ppermute x0 -> x3, waiting for transfers between devices: none -> 76.8 us  [local(): lax.ppermute(ring[-1], 'tp', [(dev, (dev + 1) % 4) for dev in range(4)])]
    all_gather x1 -> x0, waiting for transfers between devices: 57.4 us -> none  [local(): slot_rows = lax.all_gather(arrived[None], 'tp', axis=0, tiled=True)]
    unnamed x23 -> x36, local copies, waits for them, and re-layouts: 2.13 us -> 20.7 us
    dynamic_slice x0 -> x1, local copies, waits for them, and re-layouts: none -> 8.35 us  [local(): jnp.roll(jnp.concatenate(ring[::-1], axis=0), (lax.axis_index('tp') + 1)...]
  transfers between devices with their start and end apart: 3 -> 5, of which waited for: 2 -> 4; matrix products, arithmetic and copies ran while one was open for 4% -> 3% of each run, Pallas kernels for 0% -> 0%
where the time goes in v1:
time: 378 us; the launch traced here: 376 us
  blocking collectives  126 us (33%)
  waiting for transfers between devices  120 us (32%)
  local copies, waits for them, and re-layouts  78.3 us (21%)
  matrix products  19.5 us (5%)
  between operations  14.4 us (4%)
  other arithmetic  10.6 us (3%)
  starting transfers between devices  6.73 us (2%)
    ppermute x3, waiting for transfers between devices, local(): lax.ppermute(ring[-1], 'tp', [(dev, (dev + 1) % 4) for dev in range(4)])  76.8 us
    all_to_all x1, blocking collectives, local(): lax.all_to_all(outgoing, 'ep', split_axis=0, concat_axis=0, tiled=True)  55.3 us
    all_to_all x1, waiting for transfers between devices, local(): lax.all_to_all(summed, 'ep', split_axis=1, concat_axis=1, tiled=True)[0]  43 us
    scatter x1, local copies, waits for them, and re-layouts, fill_slots(): return (blank_slots.at[block_routes, slot_ids].set(copies), slot_ids)  33.4 us
    all_gather x1, blocking collectives, local(): value_piece = lax.all_gather(values, 'ep', axis=0, tiled=True)  31.6 us
    all_gather x1, blocking collectives, local(): key_piece = lax.all_gather(keys, 'ep', axis=0, tiled=True)  31.2 us
    unnamed x36, local copies, waits for them, and re-layouts  20.7 us
    dynamic_slice x1, local copies, waits for them, and re-layouts, local(): jnp.roll(jnp.concatenate(ring[::-1], axis=0), (lax.axis_index('tp') + 1)...  8.35 us
  transfers between devices with their start and end apart: 5, of which 4 were waited for; matrix products, arithmetic and copies ran while one was open for 3% of the time, Pallas kernels for 0%

profile of v1, /device:TPU:0, one launch (start us, length us, event | category | flops | bytes accessed | tf_op | source)
XLA Modules:
  0.0 376.3 jit_solution(12243224926325539768)
XLA Ops:
  7.2 0.8 constant_dynamic-slice_fusion.1
  8.4 0.6 reduce-window.6
  9.7 1.2 fusion.24
  10.9 1.3 fusion.26
  12.2 0.6 broadcast_in_dim.60
  12.8 1.2 reshape.233
  14.3 33.4 %scatter_fusion = bf16[8,64,2048]{2,1,0:T(8,128)(2,1)S(1)} fusion(bf16[8,64,2048]{2,1,0:T(8,128)(2,1)S(1)} %broadcast_in_dim.58, s32[256]{0:T(256)S(1)} %reshape.231, bf16[256,2048]{1,0:T(8,128)(2,1)} %reshape.233), kind=kCustom, calls=%fused_computation.1 | custom fusion | bytes 3147776 | tf_op jit(solution)/shard_map/scatter | solution.py:27
  47.7 55.3 %all_to_all.25 = bf16[8,64,2048]{2,1,0:T(8,128)(2,1)S(1)} all-to-all(bf16[8,64,2048]{2,1,0:T(8,128)(2,1)S(1)} %scatter_fusion), channel_id=1, replica_groups=mesh['ep'=8,'tp'=4] {'ep'}, dimensions={0} | all-to-all | bytes 4194304 | tf_op jit(solution)/shard_map/all_to_all | solution.py:139
  103.0 1.3 copy-done.2
  104.3 25.5 %collective-permute-done = bf16[1,8,64,2048]{3,2,1,0:T(8,128)(2,1)S(1)} collective-permute-done((bf16[1,8,64,2048]{3,2,1,0:T(8,128)(2,1)S(1)}, bf16[1,8,64,2048]{3,2,1,0:T(8,128)(2,1)S(1)}, u32[]{:S(2)}, u32[]{:S(2)}) %collective-permute-start) | collective-permute-done | bytes 2097184 | tf_op jit(solution)/shard_map/ppermute | solution.py:142
  129.8 25.6 %collective-permute-done.1 = bf16[1,8,64,2048]{3,2,1,0:T(8,128)(2,1)} collective-permute-done((bf16[1,8,64,2048]{3,2,1,0:T(8,128)(2,1)S(1)}, bf16[1,8,64,2048]{3,2,1,0:T(8,128)(2,1)}, u32[]{:S(2)}, u32[]{:S(2)}) %collective-permute-start.1) | collective-permute-done | bytes 2097184 | tf_op jit(solution)/shard_map/ppermute | solution.py:142
  155.3 25.8 %collective-permute-done.2 = bf16[1,8,64,2048]{3,2,1,0:T(8,128)(2,1)} collective-permute-done((bf16[1,8,64,2048]{3,2,1,0:T(8,128)(2,1)}, bf16[1,8,64,2048]{3,2,1,0:T(8,128)(2,1)}, u32[]{:S(2)}, u32[]{:S(2)}) %collective-permute-start.2) | collective-permute-done | bytes 2097184 | tf_op jit(solution)/shard_map/ppermute | solution.py:142
  181.1 3.2 constant_dynamic-update-slice_fusion.7
  184.3 3.3 constant_dynamic-update-slice_fusion.6
  187.6 1.5 constant_dynamic-update-slice_fusion.5
  189.1 1.5 constant_dynamic-update-slice_fusion.4
  190.5 3.2 constant_dynamic-update-slice_fusion.3
  193.8 3.1 constant_dynamic-update-slice_fusion.2
  196.9 1.5 constant_dynamic-update-slice_fusion.1
  198.4 1.5 constant_dynamic-update-slice_fusion
  199.9 8.4 %constant_dynamic-slice_fusion = bf16[4,8,64,2048]{3,2,1,0:T(8,128)(2,1)} fusion(bf16[8,8,64,2048]{3,2,1,0:T(8,128)(2,1)} %constant_dynamic-update-slice_fusion, s32[]{:T(128)S(6)} %select_n.43), kind=kLoop, calls=%fused_computation.78 | loop fusion | bytes 16777220 | tf_op jit(solution)/shard_map/jit(_roll_dynamic)/dynamic_slice | solution.py:143
  208.2 6.0 %fusion.29 = f32[2048,256]{1,0:T(8,128)S(1)} fusion(bf16[2048,2048]{1,0:T(8,128)(2,1)} %bitcast.131, bf16[1,2048,256]{2,1,0:T(8,128)(2,1)S(1)} %copy-done.10), kind=kOutput, calls=%fused_computation.40 | convolution fusion | flops 2147483648 | bytes 11534336 | tf_op jit(solution)/shard_map/dot_general | solution.py:147
  214.3 2.8 fusion.23
  217.0 5.6 %convolution_convert_fusion = bf16[4,8,64,2048]{3,2,1,0:T(8,128)(2,1)} fusion(bf16[4,8,64,256]{3,2,1,0:T(8,128)(2,1)S(1)} %bitcast.136, bf16[1,256,2048]{2,1,0:T(8,128)(2,1)S(1)} %copy-done), kind=kOutput, calls=%fused_computation.28 | convolution fusion | flops 2151677952 | bytes 10485760 | tf_op jit(solution)/shard_map/dot_general | solution.py:156
  222.7 0.8 copy-done.6
  223.5 31.2 %all_gather.6 = bf16[2048,1,128]{2,0,1:T(8,128)(2,1)S(1)} all-gather(bf16[256,1,128]{2,0,1:T(8,128)(2,1)S(1)} %copy-done.6), channel_id=1, replica_groups=mesh['ep'=8,'tp'=4] {'ep'}, dimensions={0}, use_global_device_ids=true | all-gather | bytes 589824 | tf_op jit(solution)/shard_map/all_gather | solution.py:60
  254.7 0.4 reshape.241
  255.1 0.7 copy.64
  255.9 31.6 %all_gather.7 = bf16[2048,1,128]{2,0,1:T(8,128)(2,1)S(1)} all-gather(bf16[256,1,128]{2,0,1:T(8,128)(2,1)S(1)} %copy-done.7), channel_id=1, replica_groups=mesh['ep'=8,'tp'=4] {'ep'}, dimensions={0}, use_global_device_ids=true | all-gather | bytes 589824 | tf_op jit(solution)/shard_map/all_gather | solution.py:61
  288.0 5.6 %while.15 = (s32[]{:T(128)}, f32[256,1,2,2]{0,2,3,1:T(2,128)S(1)}, f32[256,1,2,2]{0,2,3,1:T(2,128)S(1)}, f32[256,1,2,2,128]{0,4,3,2,1:T(8,128)S(1)}, s32[2]{0:T(...) while((s32[]{:T(128)}, f32[256,1,2,2]{0,2,3,1:T(2,128)S(1)}, ...), condition=%wide.region_5.6_spmd.clone, body=%wide.region_0.5_spmd.clone.sunk | while | flops 411570432 | bytes 15155487 | solution.py:104
  288.0 0.6 dynamic_slice.56
  289.1 3.3 conditional.3
  289.1 0.6 iota_add_fusion
  289.9 0.9 fusion.4
  290.8 1.0 fusion.5
  291.8 0.5 fusion.11
  292.4 0.6 dynamic_slice.56
  293.9 0.7 broadcast_divide_fusion
  294.7 0.4 fusion.33
  295.2 0.4 fusion.37
  295.6 7.6 %all_to_all.26 = bf16[256,2,128]{2,1,0:T(2,128)(2,1)S(1)} all-to-all(bf16[256,2,128]{2,1,0:T(2,128)(2,1)S(1)} %fusion.37), channel_id=1, replica_groups=mesh['ep'=8,'tp'=4] {'tp'}, dimensions={0} | all-to-all | bytes 262144 | tf_op jit(solution)/shard_map/all_to_all | solution.py:114
  303.2 6.7 %all-to-all-start.2 = ((bf16[1,8,64,2048]{3,2,0,1:T(8,128)(2,1)}), bf16[1,8,64,2048]{3,2,0,1:T(8,128)(2,1)S(1)}, u32[]{:S(2)}, u32[]{:S(2)}) async-start(bf16[1,8,64,2048]{3,2,0,1:T(8,128)(2,1)} %bitcast.133), calls=%async_computation.3 | async-start | bytes 4194304 | tf_op jit(solution)/shard_map/all_to_all | solution.py:163
  310.1 0.7 constant_dynamic-slice_fusion.2
  311.1 3.7 convolution_convert_fusion.1
  314.8 43.0 %all-to-all-done.2 = bf16[1,8,64,2048]{3,2,0,1:T(8,128)(2,1)S(1)} async-done(((bf16[1,8,64,2048]{3,2,0,1:T(8,128)(2,1)}), bf16[1,8,64,2048]{3,2,0,1:T(8,128)(2,1)S(1)}, u32[]{:S(2)}, u32[]{:S(2)}) %all-to-all-start.2) | async-done | bytes 2097184 | tf_op jit(solution)/shard_map/all_to_all | solution.py:163
  357.8 5.3 %gather_fusion = bf16[256,2048]{1,0:T(8,128)(2,1)} fusion(bf16[8,64,2048]{2,1,0:T(8,128)(2,1)S(1)} %bitcast.129, s32[256]{0:T(256)S(1)} %reshape.225), kind=kCustom, calls=%fused_computation | custom fusion | bytes 2099200 | tf_op jit(solution)/shard_map/gather | solution.py:164
  363.1 2.4 reshape.237
  365.5 3.9 %multiply_reduce_fusion = bf16[128,2048]{1,0:T(8,128)(2,1)} fusion(f32[128,2,2048]{2,1,0:T(2,128)S(1)} %reshape.237, f32[128,2]{1,0:T(8,128)S(1)} %copy.73), kind=kLoop, calls=%fused_computation.32 | loop fusion | flops 786432 | bytes 2622464 | tf_op jit(solution)/shard_map/reduce_sum | solution.py:165
  (65 shorter events, 3.0 us)
Async XLA Ops:
  7.2 209.9 %copy-start = (bf16[1,256,2048]{2,1,0:T(8,128)(2,1)S(1)}, bf16[1,256,2048]{2,1,0:T(8,128)(2,1)}, u32[]{:S(2)}) copy-start(bf16[1,256,2048]{2,1,0:T(8,128)(2,1)} %param.29) | copy-start | bytes 3145732
  7.2 296.1 %reduce-scatter.2.cloned.1.call-start = ((), (), s32[]{:S(2)}) async-start(), calls=%async_computation.4 | async-start | bytes 10485760 | tf_op jit(solution)/shard_map/reduce_scatter | solution.py:155
  103.0 1.3 copy-start.2
  104.3 25.5 %collective-permute-start = (bf16[1,8,64,2048]{3,2,1,0:T(8,128)(2,1)S(1)}, bf16[1,8,64,2048]{3,2,1,0:T(8,128)(2,1)S(1)}, u32[]{:S(2)}, u32[]{:S(2)}) collective-permute-start(bf16[1,8,64,2048]{3,2,1,0:T(8,128)(2,1)S(1)} %bitcast.130), channel_id=1, source_target_pairs={{0,1},{1,2},{2,3},{3,0},{4,5},{5,6},{6,7},{7,4},{8,9},{9,10},{10,1... | collective-permute-start | bytes 6291464 | tf_op jit(solution)/shard_map/ppermute | solution.py:142
  129.8 25.6 %collective-permute-start.1 = (bf16[1,8,64,2048]{3,2,1,0:T(8,128)(2,1)S(1)}, bf16[1,8,64,2048]{3,2,1,0:T(8,128)(2,1)}, u32[]{:S(2)}, u32[]{:S(2)}) collective-permute-start(bf16[1,8,64,2048]{3,2,1,0:T(8,128)(2,1)S(1)} %collective-permute-done), channel_id=1, source_target_pairs={{0,1},{1,2},{2,3},{3,0},{4,5},{5,6},{6,7},{7,4},{8,9},{9,10},{10,1... | collective-permute-start | bytes 6291464 | tf_op jit(solution)/shard_map/ppermute | solution.py:142
  155.3 25.8 %collective-permute-start.2 = (bf16[1,8,64,2048]{3,2,1,0:T(8,128)(2,1)}, bf16[1,8,64,2048]{3,2,1,0:T(8,128)(2,1)}, u32[]{:S(2)}, u32[]{:S(2)}) collective-permute-start(bf16[1,8,64,2048]{3,2,1,0:T(8,128)(2,1)} %collective-permute-done.1), channel_id=1, source_target_pairs={{0,1},{1,2},{2,3},{3,0},{4,5},{5,6},{6,7},{7,4},{8,9},{9,10},{10,1... | collective-permute-start | bytes 6291464 | tf_op jit(solution)/shard_map/ppermute | solution.py:142
  184.3 4.8 %copy-start.3 = (bf16[8,64,2048]{2,1,0:T(8,128)(2,1)S(1)}, bf16[8,64,2048]{2,1,0:T(8,128)(2,1)}, u32[]{:S(2)}) copy-start(bf16[8,64,2048]{2,1,0:T(8,128)(2,1)} %copy-done.2) | copy-start | bytes 6291460
  199.9 8.4 %copy-start.10 = (bf16[1,2048,256]{2,1,0:T(8,128)(2,1)S(1)}, bf16[1,2048,256]{2,1,0:T(8,128)(2,1)}, u32[]{:S(2)}) copy-start(bf16[1,2048,256]{2,1,0:T(8,128)(2,1)} %param.27) | copy-start | bytes 3145732
  208.2 6.0 %copy-start.4 = (bf16[4,8,64,2048]{3,2,1,0:T(8,128)(2,1)S(1)}, bf16[4,8,64,2048]{3,2,1,0:T(8,128)(2,1)}, u32[]{:S(2)}) copy-start(bf16[4,8,64,2048]{3,2,1,0:T(8,128)(2,1)} %constant_dynamic-slice_fusion) | copy-start | bytes 25165828
  208.2 6.0 %copy-start.11 = (bf16[1,2048,256]{2,1,0:T(8,128)(2,1)S(1)}, bf16[1,2048,256]{2,1,0:T(8,128)(2,1)}, u32[]{:S(2)}) copy-start(bf16[1,2048,256]{2,1,0:T(8,128)(2,1)} %param.28) | copy-start | bytes 3145732
  222.6 0.8 copy-start.6
  222.6 33.3 %copy-start.7 = (bf16[256,1,128]{2,0,1:T(8,128)(2,1)S(1)}, bf16[256,1,128]{2,0,1:T(8,128)(2,1)}, u32[]{:S(2)}) copy-start(bf16[256,1,128]{2,0,1:T(8,128)(2,1)} %param.19) | copy-start | bytes 196612
  222.6 65.1 %copy-start.5 = (bf16[256,2,128]{2,1,0:T(2,128)(2,1)S(1)}, bf16[256,2,128]{2,1,0:T(2,128)(2,1)}, u32[]{:S(2)}) copy-start(bf16[256,2,128]{2,1,0:T(2,128)(2,1)} %param.17) | copy-start | bytes 393220
  288.0 6.7 %copy-start.8 = (f32[2]{0:T(128)S(1)}, f32[2]{0:T(128)}, u32[]{:S(2)}) copy-start(f32[2]{0:T(128)} %param.20) | copy-start | bytes 28
  288.0 7.2 %copy-start.9 = (f32[128]{0:T(128)S(1)}, f32[128]{0:T(128)}, u32[]{:S(2)}) copy-start(f32[128]{0:T(128)} %param.21) | copy-start | bytes 1540
  303.2 54.6 %all-to-all-start.2 = ((bf16[1,8,64,2048]{3,2,0,1:T(8,128)(2,1)}), bf16[1,8,64,2048]{3,2,0,1:T(8,128)(2,1)S(1)}, u32[]{:S(2)}, u32[]{:S(2)}) async-start(bf16[1,8,64,2048]{3,2,0,1:T(8,128)(2,1)} %bitcast.133), calls=%async_computation.3 | async-start | bytes 4194304 | tf_op jit(solution)/shard_map/all_to_all | solution.py:163
  357.8 11.6 %copy-start.1 = (bf16[1,256,2048]{2,1,0:T(8,128)(2,1)S(1)}, bf16[1,256,2048]{2,1,0:T(8,128)(2,1)}, u32[]{:S(2)}) copy-start(bf16[1,256,2048]{2,1,0:T(8,128)(2,1)} %param.29) | copy-start | bytes 3145732
Sparse Core Ops, SparseCore 0:
  222.8 70.4 reduce-scatter.1
